TPU v7x, 32 devices: a whole 2x2x4 slice. The times are simulated.
32 devices in a mesh: ep: 4 (over y, x), tp: 8 (over z, core).
Axes of the slice: x: 2, y: 2, z: 4, core: 2. Of those that a mesh axis runs over, the one named last changes fastest.
Arguments:
- queries: bfloat16 [3072, 2048], P('ep', 'tp'), may hold values from -6 to 6
- keys: bfloat16 [3072, 512], P('ep'), may hold values from -6 to 6
- values: bfloat16 [3072, 512], P('ep'), may hold values from -6 to 6
- query_gain: float32 [128], replicated, may hold values from 1 to 4.5
- key_gain: float32 [128], replicated, may hold values from 1 to 4.5
- out_weight: bfloat16 [2048, 2048], P('tp'), may hold values from -0.75 to 0.75
- tokens_b: bfloat16 [1536, 2048], P('ep'), may hold values from -6 to 6
- norm_gain: float32 [2048], replicated, may hold values from 0.1 to 1.9
- routes: int32 [1536, 2], P('ep'), may hold values from 0 to 15, all different within a row; in each aligned block of 48 rows (0 to 47, 48 to 95, ...) at most 8 rows name the same one
- route_weight: float32 [1536, 2], P('ep'), may hold values from 0.2 to 1
- gate_weight: bfloat16 [16, 2048, 4096], P('ep', None, 'tp'), may hold values from -0.125 to 0.125
- up_weight: bfloat16 [16, 2048, 4096], P('ep', None, 'tp'), may hold values from -0.125 to 0.125
- down_weight: bfloat16 [16, 4096, 2048], P('ep', 'tp'), may hold values from -0.09375 to 0.09375
Outputs:
- mixed_out: bfloat16 [3072, 2048], P(('ep', 'tp'))
- expert_out: bfloat16 [1536, 2048], P(('ep', 'tp'))
Inputs may be any that keep to these rules, and one draw needn't show every extreme that they name: `routes`: A row names 2 different experts. In each aligned block of 48 rows no expert is named more than 8 times, a bound that some block reaches.
All inputs are finite; a program needn't handle non-finite values.
Results may differ from a plain program's by a relative error of at most 0.019.
Values may be sent and summed in bfloat16 or wider, within the bound.
No kernel may reach another device: no remote copies, remote signals or barrier semaphores. Data moves between devices by JAX's collectives and lax.ppermute only.
A program may use at most 128 MiB of HBM per device.

v0:
```python
import jax
import jax.numpy as jnp
from jax import lax
from jax.sharding import PartitionSpec as P

D = 2048
HD = 128
HQ = 16
KVH = 4
EXPERTS = 16
TOPK = 2
GRID_W = 64
CAP = 8
EPS = 1e-06
THETA = 10000.0


def rotate(field, positions):
    n_freq = HD // 4
    row_pos = (positions // GRID_W).astype(jnp.float32)
    col_pos = (positions % GRID_W).astype(jnp.float32)
    inverse = THETA ** (-jnp.arange(n_freq, dtype=jnp.float32) / n_freq)
    angles = jnp.stack([row_pos[:, None] * inverse, col_pos[:, None] * inverse], axis=1)
    cosine = jnp.cos(angles)[:, None]
    sine = jnp.sin(angles)[:, None]
    length, n_heads = (field.shape[0], field.shape[1])
    halves = field.reshape(length, n_heads, 2, 2, n_freq)
    leading = halves[..., 0, :]
    second = halves[..., 1, :]
    turned = jnp.stack(
        [leading * cosine - second * sine, second * cosine + leading * sine], axis=-2
    )
    return turned.reshape(length, n_heads, HD)


def prepare(source, gain_vec, positions, n_heads):
    length = source.shape[0]
    field = source.astype(jnp.float32).reshape(length, n_heads, HD)
    field = field * lax.rsqrt(jnp.mean(field * field, axis=-1, keepdims=True) + EPS) * gain_vec
    return rotate(field, positions).astype(jnp.bfloat16)


def token_mixer(queries, keys, values, query_gain, key_gain, out_weight):
    n_rows = queries.shape[0]
    q_heads = queries.shape[1] // HD
    positions = lax.axis_index("ep") * n_rows + jnp.arange(n_rows, dtype=jnp.int32)
    query_n = prepare(queries, query_gain, positions, q_heads).reshape(n_rows * q_heads, HD)
    kv_index = lax.axis_index("tp") * q_heads // (HQ // KVH)
    own_keys = prepare(
        lax.dynamic_slice_in_dim(keys, kv_index * HD, HD, 1), key_gain, positions, 1
    ).reshape(n_rows, HD)
    own_values = lax.dynamic_slice_in_dim(values, kv_index * HD, HD, 1)
    score_scale = HD ** (-0.5)
    start_state = (
        jnp.full((n_rows * q_heads,), -1e30, jnp.float32),
        jnp.zeros((n_rows * q_heads,), jnp.float32),
        jnp.zeros((n_rows * q_heads, HD), jnp.float32),
    )
    key_piece = lax.all_gather(own_keys, "ep", axis=0, tiled=True)
    value_piece = lax.all_gather(own_values, "ep", axis=0, tiled=True)
    steps_n = key_piece.shape[0] // n_rows

    def one_block(index_b, state):
        running_max, totals, numerator = state
        key_blk = lax.dynamic_slice_in_dim(key_piece, index_b * n_rows, n_rows, 0)
        value_blk = lax.dynamic_slice_in_dim(value_piece, index_b * n_rows, n_rows, 0)
        scores = (
            jnp.einsum("qd,sd->qs", query_n, key_blk, preferred_element_type=jnp.float32)
            * score_scale
        )
        new_max = jnp.maximum(running_max, jnp.max(scores, axis=1))
        shrink = jnp.exp(running_max - new_max)
        weights = jnp.exp(scores - new_max[:, None])
        totals = totals * shrink + jnp.sum(weights, axis=1)
        numerator = numerator * shrink[:, None] + jnp.dot(
            weights.astype(jnp.bfloat16), value_blk, preferred_element_type=jnp.float32
        )
        return (new_max, totals, numerator)

    running_max, totals, numerator = lax.fori_loop(0, steps_n, one_block, start_state)
    attended = (numerator / totals[:, None]).astype(jnp.bfloat16).reshape(n_rows, q_heads * HD)
    return lax.psum_scatter(
        jnp.dot(attended, out_weight, preferred_element_type=jnp.float32).astype(jnp.bfloat16),
        "tp",
        scatter_dimension=0,
        tiled=True,
    )


def expert_half(tokens_b, norm_gain, routes, route_weight, gate_weight, up_weight, down_weight):
    n_tp = lax.axis_size("tp")
    n_ep = lax.axis_size("ep")
    tp_index = lax.axis_index("tp")
    local_rows = tokens_b.shape[0]
    block_rows = local_rows // n_tp
    picks = block_rows * TOPK
    local_experts = gate_weight.shape[0]
    assigned = routes.reshape(n_tp, picks)
    onehot = (assigned[:, :, None] == jnp.arange(EXPERTS, dtype=jnp.int32)[None, None, :]).astype(
        jnp.int32
    )
    slot_rank = jnp.sum((jnp.cumsum(onehot, axis=1) - onehot) * onehot, axis=-1)
    target = assigned * CAP + slot_rank
    target_hot = (
        target[:, :, None] == jnp.arange(EXPERTS * CAP, dtype=jnp.int32)[None, None, :]
    ).astype(jnp.float32)
    token_hot = (
        jnp.arange(picks, dtype=jnp.int32)[:, None] // TOPK
        == jnp.arange(block_rows, dtype=jnp.int32)[None, :]
    ).astype(jnp.float32)
    field = tokens_b.astype(jnp.float32)
    normed = (
        field * lax.rsqrt(jnp.mean(field * field, axis=-1, keepdims=True) + EPS) * norm_gain
    ).astype(jnp.bfloat16)
    dispatch_mat = jnp.einsum(
        "baj,at->bjt", target_hot, token_hot, precision=lax.Precision.HIGHEST
    ).astype(jnp.bfloat16)
    outgoing = jnp.einsum(
        "bjt,btd->bjd",
        dispatch_mat,
        normed.reshape(n_tp, block_rows, D),
        preferred_element_type=jnp.float32,
    )
    outgoing = outgoing.astype(jnp.bfloat16).reshape(n_tp, EXPERTS, CAP, D)
    arrived = lax.all_to_all(outgoing, "ep", split_axis=1, concat_axis=2, tiled=True)
    flat_rows = arrived.reshape(-1, D)
    share_rows = flat_rows.shape[0] // n_tp
    expert_slab_rows = flat_rows.reshape(
        share_rows * lax.axis_size("tp") // share_rows, local_experts, n_ep * CAP, D
    )
    gate_act = jnp.einsum(
        "blmd,ldf->blmf", expert_slab_rows, gate_weight, preferred_element_type=jnp.float32
    )
    up_act = jnp.einsum(
        "blmd,ldf->blmf", expert_slab_rows, up_weight, preferred_element_type=jnp.float32
    )
    hidden = (jax.nn.silu(gate_act) * up_act).astype(jnp.bfloat16)
    result = jnp.einsum("blmf,lfd->blmd", hidden, down_weight, preferred_element_type=jnp.float32)
    summed = lax.psum_scatter(
        result.reshape(-1, D).astype(jnp.bfloat16), "tp", scatter_dimension=0, tiled=True
    )
    returned = lax.all_to_all(
        summed.reshape(local_experts, n_ep, CAP, D), "ep", split_axis=1, concat_axis=0, tiled=True
    )
    returned = returned.reshape(EXPERTS * CAP, D)
    own_target = lax.dynamic_index_in_dim(target_hot, tp_index, 0, keepdims=False)
    shares = (route_weight / jnp.sum(route_weight, axis=-1, keepdims=True)).reshape(n_tp, picks)
    own_shares = lax.dynamic_index_in_dim(shares, tp_index, 0, keepdims=False)
    combine = jnp.einsum(
        "at,aj->tj", token_hot, own_target * own_shares[:, None], precision=lax.Precision.HIGHEST
    )
    return jnp.dot(combine, returned.astype(jnp.float32), precision=lax.Precision.HIGHEST).astype(
        jnp.bfloat16
    )


def on_device(
    queries,
    keys,
    values,
    query_gain,
    key_gain,
    out_weight,
    tokens_b,
    norm_gain,
    routes,
    route_weight,
    gate_weight,
    up_weight,
    down_weight,
):
    mixed_out = token_mixer(queries, keys, values, query_gain, key_gain, out_weight)
    expert_out = expert_half(
        tokens_b, norm_gain, routes, route_weight, gate_weight, up_weight, down_weight
    )
    return (mixed_out, expert_out)


def solution(mesh):
    placed = (
        P("ep", "tp"),
        P("ep", None),
        P("ep", None),
        P(),
        P(),
        P("tp", None),
        P("ep", None),
        P(),
        P("ep", None),
        P("ep", None),
        P("ep", None, "tp"),
        P("ep", None, "tp"),
        P("ep", "tp", None),
    )
    return jax.shard_map(
        on_device,
        mesh=mesh,
        in_specs=placed,
        out_specs=(P(("ep", "tp"), None), P(("ep", "tp"), None)),
        check_vma=False,
    )
```

profile of v0, /device:TPU:0, one launch (start us, length us, event | category | flops | bytes accessed | tf_op | source)
XLA Modules:
  0.0 199.7 jit_solution(16089087401707294677)
XLA Ops:
  7.2 0.0 copy-start
  7.2 1.9 fusion.24
  9.1 0.8 copy.47
  9.9 0.1 reshape.432
  10.0 0.1 copy.48
  10.1 1.9 select_reduce_fusion
  12.1 0.1 copy.49
  12.1 0.3 convolution_convert_fusion.2
  12.5 1.8 fusion.26
  14.3 1.3 convert_bitcast_fusion.1
  15.6 2.3 %copy.51 = bf16[8,16,8,2048]{3,2,0,1:T(8,128)(2,1)} copy(bf16[8,16,8,2048]{3,2,1,0:T(8,128)(2,1)S(1)} %convert_bitcast_fusion.1) | data formatting | bytes 8388608 | tf_op jit(solution)/shard_map/reshape | solution.py:124
  17.9 5.3 %all-to-all-start = ((bf16[8,16,8,2048]{3,2,0,1:T(8,128)(2,1)}), bf16[8,16,8,2048]{3,2,0,1:T(8,128)(2,1)}, u32[]{:S(2)}, u32[]{:S(2)}) async-start(bf16[8,16,8,2048]{3,2,0,1:T(8,128)(2,1)} %copy.51), calls=%async_computation.1 | async-start | bytes 8388608 | tf_op jit(solution)/shard_map/all_to_all | solution.py:125
  23.2 0.1 mul.305
  23.3 0.0 copy-done.1
  23.3 0.2 copy.44
  23.5 0.1 broadcast_multiply_fusion.1
  23.6 0.7 fusion.48
  24.3 0.1 bitcast_reduce_fusion
  24.4 0.1 multiply_multiply_fusion
  24.5 0.1 subtract_convert_fusion
  24.7 47.1 %all-to-all-done = bf16[8,16,8,2048]{3,2,0,1:T(8,128)(2,1)} async-done(((bf16[8,16,8,2048]{3,2,0,1:T(8,128)(2,1)}), bf16[8,16,8,2048]{3,2,0,1:T(8,128)(2,1)}, u32[]{:S(2)}, u32[]{:S(2)}) %all-to-all-start) | async-done | bytes 4194336 | tf_op jit(solution)/shard_map/all_to_all | solution.py:125
  71.8 8.4 %fusion.16 = f32[4,8,32,512]{3,2,1,0:T(8,128)} fusion(bf16[4,2048,512]{2,1,0:T(8,128)(2,1)} %param.25, bf16[8,4,4,8,2048]{4,3,0,2,1:T(8,128)(2,1)} %bitcast.11), kind=kOutput, calls=%fused_computation.22 | convolution fusion | flops 2147483648 | bytes 14680064 | tf_op jit(solution)/shard_map/blmd,ldf->blmf/dot_general | solution.py:131
  80.2 14.2 %convert_bitcast_fusion = bf16[8,4,32,2048]{3,2,0,1:T(8,128)(2,1)} fusion(bf16[4,512,2048]{2,1,0:T(8,128)(2,1)} %param.27, f32[4,8,32,512]{3,2,1,0:T(8,128)} %fusion.16, bf16[4,2048,512]{2,1,0:T(8,128)(2,1)} %param.26, bf16[8,4,4,8,2048]{4,3,0,2,1:T(8,128)(2,1)} %bitcast.11), kind=kOutput, calls=%fused_computation.26 | convolution fusion | flops 4300210176 | bytes 27262976 | tf_op jit(solution)/shard_map/blmf,lfd->blmd/dot_general | solution.py:138
  94.4 4.7 %copy.53 = bf16[8,4,32,2048]{3,2,1,0:T(8,128)(2,1)} copy(bf16[8,4,32,2048]{3,2,0,1:T(8,128)(2,1)} %convert_bitcast_fusion) | data formatting | bytes 8388608 | tf_op jit(solution)/shard_map/convert_element_type | solution.py:140
  99.1 0.0 reduce-scatter.5.cloned.1.call-update
  99.1 0.2 reduce-scatter.3.cloned.1.call-start
  99.3 0.9 constant_dynamic-slice_fusion.2
  100.3 0.1 copy.59
  100.5 2.9 %copy.45 = bf16[768,2,2,2,32]{4,3,2,1,0:T(2,128)(2,1)} copy(bf16[768,2,2,2,32]{0,4,3,2,1:T(8,128)(2,1)S(1)} %pad_maximum_fusion) | data formatting | bytes 786432 | tf_op jit(solution)/shard_map/stack | solution.py:30
  103.4 3.7 %convert_element_type.88 = bf16[1536,128]{1,0:T(8,128)(2,1)S(1)} reshape(bf16[768,2,2,2,32]{4,3,2,1,0:T(2,128)(2,1)} %copy.45) | data formatting | bytes 786432 | tf_op jit(solution)/shard_map/convert_element_type | solution.py:40
  107.1 0.9 constant_dynamic-slice_fusion.1
  108.0 0.1 fusion.44
  108.1 0.1 fusion.45
  108.2 0.7 subtract_convert_fusion.1
  109.0 12.7 %all_gather.6 = bf16[3072,128]{0,1:T(8,128)(2,1)S(1)} all-gather(bf16[768,128]{0,1:T(8,128)(2,1)S(1)} %bitcast.98), channel_id=1, replica_groups=mesh['ep'=4,'tp'=8] {'ep'}, dimensions={0}, use_global_device_ids=true | all-gather | bytes 983040 | tf_op jit(solution)/shard_map/all_gather | solution.py:59
  121.7 11.2 %all_gather.7 = bf16[3072,128]{1,0:T(8,128)(2,1)} all-gather(bf16[768,128]{1,0:T(8,128)(2,1)S(1)} %constant_dynamic-slice_fusion.1), channel_id=1, replica_groups=mesh['ep'=4,'tp'=8] {'ep'}, dimensions={0}, use_global_device_ids=true | all-gather | bytes 983040 | tf_op jit(solution)/shard_map/all_gather | solution.py:60
  132.9 15.4 %while.18 = (s32[]{:T(128)}, f32[1536]{0:T(1024)S(1)}, f32[1536]{0:T(1024)S(1)}, f32[1536,128]{1,0:T(8,128)S(1)}, bf16[3072,128]{0,1:T(8,128)(2,1)S(1)}, /*index...) while((s32[]{:T(128)}, f32[1536]{0:T(1024)S(1)}, ...), condition=%wide.region_5.6_spmd.clone, body=%wide.region_2.5_spmd.clone.sunk | while | flops 614014464 | bytes 16613559 | solution.py:80
  132.9 0.8 multiply_reduce_fusion.2
  133.8 0.8 fusion.86
  134.6 2.1 %convolution_add_fusion.2 = f32[1536,128]{1,0:T(8,128)S(1)} fusion(f32[768,1536]{1,0:T(8,128)S(1)} %get-tuple-element.254, f32[1536]{0:T(1024)S(1)} %select_maximum_fusion.2, f32[1536,128]{1,0:T(8,128)S(1)} %get-tuple-element.271, f32[1536]{0:T(1024)S(1)} %get-tuple-element.256, pred[]{:T(512)S(6)} %compare.22, ...), kind=kOutput, calls=%fused_computation.4.clone.1 | convolution fusion | flops 306118656 | bytes 6500357 | tf_op jit(solution)/shard_map/while/body/eval_jaxpr/dot_general | solution.py:75
  136.8 0.8 multiply_reduce_fusion.2
  137.6 0.8 fusion.86
  138.4 2.1 %convolution_add_fusion.2 = f32[1536,128]{1,0:T(8,128)S(1)} fusion(f32[768,1536]{1,0:T(8,128)S(1)} %get-tuple-element.254, f32[1536]{0:T(1024)S(1)} %select_maximum_fusion.2, f32[1536,128]{1,0:T(8,128)S(1)} %get-tuple-element.271, f32[1536]{0:T(1024)S(1)} %get-tuple-element.256, pred[]{:T(512)S(6)} %compare.22, ...), kind=kOutput, calls=%fused_computation.4.clone.1 | convolution fusion | flops 306118656 | bytes 6500357 | tf_op jit(solution)/shard_map/while/body/eval_jaxpr/dot_general | solution.py:75
  140.6 0.8 multiply_reduce_fusion.2
  141.5 0.8 fusion.86
  142.3 2.2 %convolution_add_fusion.2 = f32[1536,128]{1,0:T(8,128)S(1)} fusion(f32[768,1536]{1,0:T(8,128)S(1)} %get-tuple-element.254, f32[1536]{0:T(1024)S(1)} %select_maximum_fusion.2, f32[1536,128]{1,0:T(8,128)S(1)} %get-tuple-element.271, f32[1536]{0:T(1024)S(1)} %get-tuple-element.256, pred[]{:T(512)S(6)} %compare.22, ...), kind=kOutput, calls=%fused_computation.4.clone.1 | convolution fusion | flops 306118656 | bytes 6500357 | tf_op jit(solution)/shard_map/while/body/eval_jaxpr/dot_general | solution.py:75
  144.5 0.8 multiply_reduce_fusion.2
  145.3 0.8 fusion.86
  146.1 2.2 %convolution_add_fusion.2 = f32[1536,128]{1,0:T(8,128)S(1)} fusion(f32[768,1536]{1,0:T(8,128)S(1)} %get-tuple-element.254, f32[1536]{0:T(1024)S(1)} %select_maximum_fusion.2, f32[1536,128]{1,0:T(8,128)S(1)} %get-tuple-element.271, f32[1536]{0:T(1024)S(1)} %get-tuple-element.256, pred[]{:T(512)S(6)} %compare.22, ...), kind=kOutput, calls=%fused_computation.4.clone.1 | convolution fusion | flops 306118656 | bytes 6500357 | tf_op jit(solution)/shard_map/while/body/eval_jaxpr/dot_general | solution.py:75
  148.3 0.3 divide_convert_fusion
  148.6 0.1 reshape.431
  148.7 0.0 copy-start.2
  148.8 2.7 %convolution_convert_fusion = bf16[768,2048]{1,0:T(8,128)(2,1)} fusion(bf16[768,256]{1,0:T(8,128)(2,1)S(1)} %reshape.431, bf16[256,2048]{1,0:T(8,128)(2,1)S(1)} %copy-done), kind=kOutput, calls=%fused_computation.32 | convolution fusion | flops 806879232 | bytes 4587520 | tf_op jit(solution)/shard_map/dot_general | solution.py:83
  151.4 0.0 reduce-scatter.3.cloned.1.call-update
  151.5 0.2 iota_compare_fusion
  151.7 0.0 reduce-scatter.5.cloned.1.call-done
  151.7 1.9 copy.54
  153.6 3.5 %all-to-all-start.1 = ((bf16[4,4,8,2048]{3,2,0,1:T(8,128)(2,1)}), bf16[4,4,8,2048]{3,2,0,1:T(8,128)(2,1)S(1)}, u32[]{:S(2)}, u32[]{:S(2)}) async-start(bf16[4,4,8,2048]{3,2,0,1:T(8,128)(2,1)} %copy.54), calls=%async_computation.3 | async-start | bytes 1048576 | tf_op jit(solution)/shard_map/all_to_all | solution.py:142
  157.1 0.1 copy.50
  157.2 0.1 reshape.433
  157.4 0.2 fusion.51
  157.6 6.0 %all-to-all-done.1 = bf16[4,4,8,2048]{3,2,0,1:T(8,128)(2,1)S(1)} async-done(((bf16[4,4,8,2048]{3,2,0,1:T(8,128)(2,1)}), bf16[4,4,8,2048]{3,2,0,1:T(8,128)(2,1)S(1)}, u32[]{:S(2)}, u32[]{:S(2)}) %all-to-all-start.1) | async-done | bytes 524320 | tf_op jit(solution)/shard_map/all_to_all | solution.py:142
  163.6 1.0 convolution_convert_fusion.1
  164.6 28.2 %reduce-scatter.3.cloned.1.call-done = bf16[96,2048]{1,0:T(8,128)(2,1)} async-done(((bf16[768,2048]{1,0:T(8,128)(2,1)}), bf16[96,2048]{1,0:T(8,128)(2,1)}) %reduce-scatter.3.cloned.1.call-update) | async-done | bytes 393232 | tf_op jit(solution)/shard_map/reduce_scatter | solution.py:82
  (35 shorter events, 0.3 us)
Async XLA Ops:
  7.2 141.6 %copy-start = (bf16[256,2048]{1,0:T(8,128)(2,1)S(1)}, bf16[256,2048]{1,0:T(8,128)(2,1)}, u32[]{:S(2)}) copy-start(bf16[256,2048]{1,0:T(8,128)(2,1)} %param.20) | copy-start | bytes 3145732
  17.9 5.3 %copy-start.3 = (f32[128]{0:T(128)S(1)}, f32[128]{0:T(128)}, u32[]{:S(2)}) copy-start(f32[128]{0:T(128)} %param.18) | copy-start | bytes 1540
  17.9 5.4 %copy-start.1 = (bf16[768,256]{1,0:T(8,128)(2,1)S(1)}, bf16[768,256]{1,0:T(8,128)(2,1)}, u32[]{:S(2)}) copy-start(bf16[768,256]{1,0:T(8,128)(2,1)} %param.15) | copy-start | bytes 1179652
  17.9 53.9 %all-to-all-start = ((bf16[8,16,8,2048]{3,2,0,1:T(8,128)(2,1)}), bf16[8,16,8,2048]{3,2,0,1:T(8,128)(2,1)}, u32[]{:S(2)}, u32[]{:S(2)}) async-start(bf16[8,16,8,2048]{3,2,0,1:T(8,128)(2,1)} %copy.51), calls=%async_computation.1 | async-start | bytes 8388608 | tf_op jit(solution)/shard_map/all_to_all | solution.py:125
  23.2 128.5 %reduce-scatter.5.cloned.1.call-start = ((), (), s32[]{:S(2)}) async-start(), calls=%async_computation.5 | async-start | bytes 4718592 | tf_op jit(solution)/shard_map/reduce_scatter | solution.py:139
  99.1 9.0 %copy-start.4 = (f32[128]{0:T(128)S(1)}, f32[128]{0:T(128)}, u32[]{:S(2)}) copy-start(f32[128]{0:T(128)} %param.19) | copy-start | bytes 1540
  99.1 93.7 %reduce-scatter.3.cloned.1.call-start = ((), (), s32[]{:S(2)}) async-start(), calls=%async_computation.4 | async-start | bytes 3538944 | tf_op jit(solution)/shard_map/reduce_scatter | solution.py:82
  148.7 2.7 %copy-start.2 = (f32[384,2]{0,1:T(2,128)S(1)}, f32[384,2]{0,1:T(2,128)}, u32[]{:S(2)}) copy-start(f32[384,2]{0,1:T(2,128)} %param.24) | copy-start | bytes 9220
  153.6 10.0 %all-to-all-start.1 = ((bf16[4,4,8,2048]{3,2,0,1:T(8,128)(2,1)}), bf16[4,4,8,2048]{3,2,0,1:T(8,128)(2,1)S(1)}, u32[]{:S(2)}, u32[]{:S(2)}) async-start(bf16[4,4,8,2048]{3,2,0,1:T(8,128)(2,1)} %copy.54), calls=%async_computation.3 | async-start | bytes 1048576 | tf_op jit(solution)/shard_map/all_to_all | solution.py:142
Sparse Core Ops, SparseCore 0:
  99.2 50.3 reduce-scatter.4
  152.6 40.2 reduce-scatter.2
where the time goes:
time: 200 us
  waiting for transfers between devices  81.4 us (41%)
  matrix products  40 us (20%)
  blocking collectives  23.9 us (12%)
  local copies, waits for them, and re-layouts  19.3 us (10%)
  between operations  14.3 us (7%)
  other arithmetic  11.5 us (6%)
  starting transfers between devices  9.02 us (5%)
    all_to_all x1, waiting for transfers between devices, expert_half(): lax.all_to_all(outgoing, 'ep', split_axis=1, concat_axis=2, tiled=True)  47.1 us
    reduce_scatter x1, waiting for transfers between devices, token_mixer(): lax.psum_scatter(jnp.dot(attended, out_weight, preferred_element_type=jnp...  28.2 us
    dot_general x1, matrix products, expert_half(): jnp.einsum('blmf,lfd->blmd', hidden, down_weight, preferred_element_type=...  14.2 us
    all_gather x1, blocking collectives, token_mixer(): key_piece = lax.all_gather(own_keys, 'ep', axis=0, tiled=True)  12.7 us
    all_gather x1, blocking collectives, token_mixer(): value_piece = lax.all_gather(own_values, 'ep', axis=0, tiled=True)  11.2 us
    dot_general x4, matrix products, one_block(): jnp.dot(weights.astype(jnp.bfloat16), value_blk, preferred_element_type=j...  8.6 us
    dot_general x1, matrix products, expert_half(): jnp.einsum('blmd,ldf->blmf', expert_slab_rows, gate_weight, preferred_ele...  8.38 us
    all_to_all x1, waiting for transfers between devices, expert_half(): lax.all_to_all(summed.reshape(local_experts, n_ep, CAP, D), 'ep', split_a...  6.01 us
  transfers between devices with their start and end apart: 4, of which 3 were waited for; matrix products, arithmetic and copies ran while one was open for 16% of the time, Pallas kernels for 0%

commit v1 on v0

--- a/solution.py
+++ b/solution.py
@@ -122,7 +122,10 @@
         preferred_element_type=jnp.float32,
     )
     outgoing = outgoing.astype(jnp.bfloat16).reshape(n_tp, EXPERTS, CAP, D)
-    arrived = lax.all_to_all(outgoing, "ep", split_axis=1, concat_axis=2, tiled=True)
+    size = lax.axis_size("ep")
+    blocks = jnp.stack(jnp.split(outgoing, size, axis=1), axis=0)
+    blocks = lax.all_to_all(blocks, "ep", split_axis=0, concat_axis=0)
+    arrived = jnp.concatenate(blocks, axis=2)
     flat_rows = arrived.reshape(-1, D)
     share_rows = flat_rows.shape[0] // n_tp
     expert_slab_rows = flat_rows.reshape(

time: 200 us -> 221 us (1.10)
  other arithmetic: 11.5 us -> 23.7 us
  matrix products: 40 us -> 48.6 us
    reduce_sum x4, other arithmetic: 3.21 us -> 13.3 us  [one_block(): totals = totals * shrink + jnp.sum(weights, axis=1)]
    dot_general x4, matrix products: 3.31 us -> 12 us  [one_block(): jnp.einsum('qd,sd->qs', query_n, key_blk, preferred_element_type=jnp.floa...]
    reshape x1 -> x0, local copies, waits for them, and re-layouts: 2.28 us -> none  [expert_half(): outgoing = outgoing.astype(jnp.bfloat16).reshape(n_tp, EXPERTS, CAP, D)]
    another operation x2 -> x3, other arithmetic: 0.83 us -> 3.07 us  [the longest x1 2.25 us: expert_half(): blocks = jnp.stack(jnp.split(outgoing, size, axis=1), axis=0)]
  transfers between devices with their start and end apart: 4 -> 4, of which waited for: 3 -> 3; matrix products, arithmetic and copies ran while one was open for 16% -> 23% of each run, Pallas kernels for 0% -> 0%
where the time goes in v1:
time: 221 us
  waiting for transfers between devices  81.3 us (37%)
  matrix products  48.6 us (22%)
  blocking collectives  24.2 us (11%)
  other arithmetic  23.7 us (11%)
  local copies, waits for them, and re-layouts  19.6 us (9%)
  between operations  14.3 us (6%)
  starting transfers between devices  8.84 us (4%)
    all_to_all x1, waiting for transfers between devices, expert_half(): blocks = lax.all_to_all(blocks, 'ep', split_axis=0, concat_axis=0)  47.1 us
    reduce_scatter x1, waiting for transfers between devices, token_mixer(): lax.psum_scatter(jnp.dot(attended, out_weight, preferred_element_type=jnp...  28.1 us
    dot_general x1, matrix products, expert_half(): jnp.einsum('blmf,lfd->blmd', hidden, down_weight, preferred_element_type=...  14.2 us
    reduce_sum x4, other arithmetic, one_block(): totals = totals * shrink + jnp.sum(weights, axis=1)  13.3 us
    all_gather x1, blocking collectives, token_mixer(): key_piece = lax.all_gather(own_keys, 'ep', axis=0, tiled=True)  12.7 us
    dot_general x4, matrix products, one_block(): jnp.einsum('qd,sd->qs', query_n, key_blk, preferred_element_type=jnp.floa...  12 us
    all_gather x1, blocking collectives, token_mixer(): value_piece = lax.all_gather(own_values, 'ep', axis=0, tiled=True)  11.4 us
    dot_general x4, matrix products, one_block(): jnp.dot(weights.astype(jnp.bfloat16), value_blk, preferred_element_type=j...  8.58 us
  transfers between devices with their start and end apart: 4, of which 3 were waited for; matrix products, arithmetic and copies ran while one was open for 23% of the time, Pallas kernels for 0%

profile of v1, /device:TPU:0, one launch (start us, length us, event | category | flops | bytes accessed | tf_op | source)
XLA Modules:
  0.0 220.7 jit_solution(18117744069012055431)
XLA Ops:
  7.2 0.9 copy.46
  8.1 0.1 reshape.435
  8.2 0.1 copy.47
  8.3 1.9 select_reduce_fusion
  10.2 0.1 copy.48
  10.3 1.8 fusion.24
  12.1 0.3 convolution_convert_fusion.2
  12.4 1.8 fusion.26
  14.3 1.3 convert_bitcast_fusion.1
  15.6 0.6 slice_bitcast_fusion.3
  16.2 2.2 %pad_maximum_fusion = bf16[4,8,4,8,2048]{4,3,2,1,0:T(8,128)(2,1)} fusion(bf16[1,8,4,8,2048]{4,3,2,1,0:T(8,128)(2,1)S(1)} %get-tuple-element.193, bf16[1,8,4,8,2048]{4,3,2,1,0:T(8,128)(2,1)S(1)} %get-tuple-element.194, bf16[1,8,4,8,2048]{4,3,2,1,0:T(8,128)(2,1)S(1)} %get-tuple-element.195, bf16[1,8,4,8,2048]{4,3,2,1,0:T(8,128)(2,1)S(1)} %get-tuple-element.192), kind=kLoop, calls=%fused_computation.24 | loop fusion | flops 6291456 | bytes 8388608 | tf_op jit(solution)/shard_map/stack | solution.py:126
  18.4 5.3 %all-to-all-start = ((bf16[4,8,4,8,2048]{4,3,2,1,0:T(8,128)(2,1)}), bf16[4,8,4,8,2048]{4,3,2,1,0:T(8,128)(2,1)}, u32[]{:S(2)}, u32[]{:S(2)}) async-start(bf16[4,8,4,8,2048]{4,3,2,1,0:T(8,128)(2,1)} %pad_maximum_fusion), calls=%async_computation.1 | async-start | bytes 8388608 | tf_op jit(solution)/shard_map/all_to_all | solution.py:127
  23.7 0.2 copy.43
  23.9 0.1 mul.305
  24.0 0.1 broadcast_multiply_fusion.1
  24.2 0.7 fusion.48
  24.8 0.1 bitcast_reduce_fusion
  25.0 0.1 multiply_multiply_fusion
  25.1 0.1 subtract_convert_fusion
  25.2 47.1 %all-to-all-done = bf16[4,8,4,8,2048]{4,3,2,1,0:T(8,128)(2,1)} async-done(((bf16[4,8,4,8,2048]{4,3,2,1,0:T(8,128)(2,1)}), bf16[4,8,4,8,2048]{4,3,2,1,0:T(8,128)(2,1)}, u32[]{:S(2)}, u32[]{:S(2)}) %all-to-all-start) | async-done | bytes 4194336 | tf_op jit(solution)/shard_map/all_to_all | solution.py:127
  72.4 8.4 %fusion.16 = f32[4,8,32,512]{3,2,1,0:T(8,128)} fusion(bf16[4,2048,512]{2,1,0:T(8,128)(2,1)} %param.25, bf16[4,8,4,8,2048]{4,3,2,1,0:T(8,128)(2,1)} %all-to-all-done), kind=kOutput, calls=%fused_computation.22 | convolution fusion | flops 2147483648 | bytes 14680064 | tf_op jit(solution)/shard_map/blmd,ldf->blmf/dot_general | solution.py:134
  80.7 14.2 %convert_bitcast_fusion = bf16[8,4,32,2048]{3,2,0,1:T(8,128)(2,1)} fusion(bf16[4,512,2048]{2,1,0:T(8,128)(2,1)} %param.27, f32[4,8,32,512]{3,2,1,0:T(8,128)} %fusion.16, bf16[4,2048,512]{2,1,0:T(8,128)(2,1)} %param.26, bf16[4,8,4,8,2048]{4,3,2,1,0:T(8,128)(2,1)} %all-to-all-done), kind=kOutput, calls=%fused_computation.27 | convolution fusion | flops 4300210176 | bytes 27262976 | tf_op jit(solution)/shard_map/blmf,lfd->blmd/dot_general | solution.py:141
  94.9 4.7 %copy.51 = bf16[8,4,32,2048]{3,2,1,0:T(8,128)(2,1)} copy(bf16[8,4,32,2048]{3,2,0,1:T(8,128)(2,1)} %convert_bitcast_fusion) | data formatting | bytes 8388608 | tf_op jit(solution)/shard_map/convert_element_type | solution.py:143
  99.7 0.0 reduce-scatter.3.cloned.1.call-start
  99.7 0.9 constant_dynamic-slice_fusion.2
  100.7 0.1 copy.57
  100.8 2.9 %copy.44 = bf16[768,2,2,2,32]{4,3,2,1,0:T(2,128)(2,1)} copy(bf16[768,2,2,2,32]{0,4,3,2,1:T(8,128)(2,1)S(1)} %pad_maximum_fusion.1) | data formatting | bytes 786432 | tf_op jit(solution)/shard_map/stack | solution.py:30
  103.8 3.7 %convert_element_type.88 = bf16[1536,128]{1,0:T(8,128)(2,1)S(1)} reshape(bf16[768,2,2,2,32]{4,3,2,1,0:T(2,128)(2,1)} %copy.44) | data formatting | bytes 786432 | tf_op jit(solution)/shard_map/convert_element_type | solution.py:40
  107.5 0.9 constant_dynamic-slice_fusion.1
  108.4 0.1 fusion.44
  108.5 0.1 fusion.45
  108.6 0.7 subtract_convert_fusion.1
  109.4 12.7 %all_gather.6 = bf16[3072,128]{0,1:T(8,128)(2,1)S(1)} all-gather(bf16[768,128]{0,1:T(8,128)(2,1)S(1)} %bitcast.111), channel_id=1, replica_groups=mesh['ep'=4,'tp'=8] {'ep'}, dimensions={0}, use_global_device_ids=true | all-gather | bytes 983040 | tf_op jit(solution)/shard_map/all_gather | solution.py:59
  122.1 11.4 %all_gather.7 = bf16[3072,128]{1,0:T(8,128)(2,1)} all-gather(bf16[768,128]{1,0:T(8,128)(2,1)S(1)} %constant_dynamic-slice_fusion.1), channel_id=1, replica_groups=mesh['ep'=4,'tp'=8] {'ep'}, dimensions={0}, use_global_device_ids=true | all-gather | bytes 983040 | tf_op jit(solution)/shard_map/all_gather | solution.py:60
  133.5 35.9 %while.18 = (s32[]{:T(128)}, f32[1536]{0:T(1024)S(1)}, f32[1536]{0:T(1024)S(1)}, f32[1536,128]{1,0:T(8,128)S(1)}, bf16[3072,128]{0,1:T(8,128)(2,1)S(1)}, /*index...) while((s32[]{:T(128)}, f32[1536]{0:T(1024)S(1)}, ...), condition=%wide.region_5.6_spmd.clone, body=%wide.region_2.5_spmd.clone.sunk | while | flops 614014464 | bytes 35487944 | solution.py:80
  133.5 3.0 %multiply_reduce_fusion.2 = (f32[1536]{0:T(1024)S(1)}, f32[768,1536]{1,0:T(8,128)}) fusion(bf16[1536,128]{1,0:T(8,128)(2,1)S(1)} %get-tuple-element.288, bf16[3072,128]{0,1:T(8,128)(2,1)S(1)} %get-tuple-element.287, s32[]{:T(128)S(6)} %select_n.72), kind=kOutput, calls=%fused_computation.1.clone.1 | convolution fusion | flops 304347648 | bytes 5314564 | tf_op jit(solution)/shard_map/while/body/eval_jaxpr/qd,sd->qs/dot_general | solution.py:68
  136.5 3.3 %fusion.88 = f32[1536]{0:T(1024)S(1)} fusion(f32[768,1536]{1,0:T(8,128)} %get-tuple-element.258, f32[1536]{0:T(1024)S(1)} %select_maximum_fusion.2), kind=kLoop, calls=%fused_computation.3.clone.1 | loop fusion | flops 3537408 | bytes 4730880 | tf_op jit(solution)/shard_map/while/body/eval_jaxpr/reduce_sum | solution.py:74
  139.9 0.5 copy-done.1
  140.4 2.1 convolution_add_fusion.2
  142.6 3.0 %multiply_reduce_fusion.2 = (f32[1536]{0:T(1024)S(1)}, f32[768,1536]{1,0:T(8,128)}) fusion(bf16[1536,128]{1,0:T(8,128)(2,1)S(1)} %get-tuple-element.288, bf16[3072,128]{0,1:T(8,128)(2,1)S(1)} %get-tuple-element.287, s32[]{:T(128)S(6)} %select_n.72), kind=kOutput, calls=%fused_computation.1.clone.1 | convolution fusion | flops 304347648 | bytes 5314564 | tf_op jit(solution)/shard_map/while/body/eval_jaxpr/qd,sd->qs/dot_general | solution.py:68
  145.6 3.3 %fusion.88 = f32[1536]{0:T(1024)S(1)} fusion(f32[768,1536]{1,0:T(8,128)} %get-tuple-element.258, f32[1536]{0:T(1024)S(1)} %select_maximum_fusion.2), kind=kLoop, calls=%fused_computation.3.clone.1 | loop fusion | flops 3537408 | bytes 4730880 | tf_op jit(solution)/shard_map/while/body/eval_jaxpr/reduce_sum | solution.py:74
  148.9 0.5 copy-done.1
  149.4 2.1 convolution_add_fusion.2
  151.6 3.0 %multiply_reduce_fusion.2 = (f32[1536]{0:T(1024)S(1)}, f32[768,1536]{1,0:T(8,128)}) fusion(bf16[1536,128]{1,0:T(8,128)(2,1)S(1)} %get-tuple-element.288, bf16[3072,128]{0,1:T(8,128)(2,1)S(1)} %get-tuple-element.287, s32[]{:T(128)S(6)} %select_n.72), kind=kOutput, calls=%fused_computation.1.clone.1 | convolution fusion | flops 304347648 | bytes 5314564 | tf_op jit(solution)/shard_map/while/body/eval_jaxpr/qd,sd->qs/dot_general | solution.py:68
  154.6 3.3 %fusion.88 = f32[1536]{0:T(1024)S(1)} fusion(f32[768,1536]{1,0:T(8,128)} %get-tuple-element.258, f32[1536]{0:T(1024)S(1)} %select_maximum_fusion.2), kind=kLoop, calls=%fused_computation.3.clone.1 | loop fusion | flops 3537408 | bytes 4730880 | tf_op jit(solution)/shard_map/while/body/eval_jaxpr/reduce_sum | solution.py:74
  157.9 0.4 copy-done.1
  158.4 2.1 convolution_add_fusion.2
  160.5 3.0 %multiply_reduce_fusion.2 = (f32[1536]{0:T(1024)S(1)}, f32[768,1536]{1,0:T(8,128)}) fusion(bf16[1536,128]{1,0:T(8,128)(2,1)S(1)} %get-tuple-element.288, bf16[3072,128]{0,1:T(8,128)(2,1)S(1)} %get-tuple-element.287, s32[]{:T(128)S(6)} %select_n.72), kind=kOutput, calls=%fused_computation.1.clone.1 | convolution fusion | flops 304347648 | bytes 5314564 | tf_op jit(solution)/shard_map/while/body/eval_jaxpr/qd,sd->qs/dot_general | solution.py:68
  163.5 3.3 %fusion.88 = f32[1536]{0:T(1024)S(1)} fusion(f32[768,1536]{1,0:T(8,128)} %get-tuple-element.258, f32[1536]{0:T(1024)S(1)} %select_maximum_fusion.2), kind=kLoop, calls=%fused_computation.3.clone.1 | loop fusion | flops 3537408 | bytes 4730880 | tf_op jit(solution)/shard_map/while/body/eval_jaxpr/reduce_sum | solution.py:74
  166.8 0.4 copy-done.1
  167.3 2.1 convolution_add_fusion.2
  169.5 0.3 divide_convert_fusion
  169.7 0.1 reshape.434
  169.9 2.7 %convolution_convert_fusion = bf16[768,2048]{1,0:T(8,128)(2,1)} fusion(bf16[768,256]{1,0:T(8,128)(2,1)S(1)} %reshape.434, bf16[256,2048]{1,0:T(8,128)(2,1)S(1)} %copy-done), kind=kOutput, calls=%fused_computation.33 | convolution fusion | flops 806879232 | bytes 4587520 | tf_op jit(solution)/shard_map/dot_general | solution.py:83
  172.6 0.2 iota_compare_fusion
  172.8 0.0 reduce-scatter.5.cloned.1.call-done
  172.8 1.9 copy.52
  174.7 3.5 %all-to-all-start.1 = ((bf16[4,4,8,2048]{3,2,0,1:T(8,128)(2,1)}), bf16[4,4,8,2048]{3,2,0,1:T(8,128)(2,1)S(1)}, u32[]{:S(2)}, u32[]{:S(2)}) async-start(bf16[4,4,8,2048]{3,2,0,1:T(8,128)(2,1)} %copy.52), calls=%async_computation.3 | async-start | bytes 1048576 | tf_op jit(solution)/shard_map/all_to_all | solution.py:145
  178.2 0.1 copy.49
  178.3 0.1 reshape.436
  178.5 0.2 fusion.51
  178.7 6.0 %all-to-all-done.1 = bf16[4,4,8,2048]{3,2,0,1:T(8,128)(2,1)S(1)} async-done(((bf16[4,4,8,2048]{3,2,0,1:T(8,128)(2,1)}), bf16[4,4,8,2048]{3,2,0,1:T(8,128)(2,1)S(1)}, u32[]{:S(2)}, u32[]{:S(2)}) %all-to-all-start.1) | async-done | bytes 524320 | tf_op jit(solution)/shard_map/all_to_all | solution.py:145
  184.7 1.0 convolution_convert_fusion.1
  185.7 28.1 %reduce-scatter.3.cloned.1.call-done = bf16[96,2048]{1,0:T(8,128)(2,1)} async-done(((bf16[768,2048]{1,0:T(8,128)(2,1)}), bf16[96,2048]{1,0:T(8,128)(2,1)}) %reduce-scatter.3.cloned.1.call-update) | async-done | bytes 393232 | tf_op jit(solution)/shard_map/reduce_scatter | solution.py:82
  (44 shorter events, 0.3 us)
Async XLA Ops:
  7.2 162.7 %copy-start = (bf16[256,2048]{1,0:T(8,128)(2,1)S(1)}, bf16[256,2048]{1,0:T(8,128)(2,1)}, u32[]{:S(2)}) copy-start(bf16[256,2048]{1,0:T(8,128)(2,1)} %param.20) | copy-start | bytes 3145732
  18.4 5.3 %copy-start.2 = (bf16[768,256]{1,0:T(8,128)(2,1)S(1)}, bf16[768,256]{1,0:T(8,128)(2,1)}, u32[]{:S(2)}) copy-start(bf16[768,256]{1,0:T(8,128)(2,1)} %param.15) | copy-start | bytes 1179652
  18.4 5.5 %copy-start.4 = (f32[128]{0:T(128)S(1)}, f32[128]{0:T(128)}, u32[]{:S(2)}) copy-start(f32[128]{0:T(128)} %param.18) | copy-start | bytes 1540
  18.4 53.9 %all-to-all-start = ((bf16[4,8,4,8,2048]{4,3,2,1,0:T(8,128)(2,1)}), bf16[4,8,4,8,2048]{4,3,2,1,0:T(8,128)(2,1)}, u32[]{:S(2)}, u32[]{:S(2)}) async-start(bf16[4,8,4,8,2048]{4,3,2,1,0:T(8,128)(2,1)} %pad_maximum_fusion), calls=%async_computation.1 | async-start | bytes 8388608 | tf_op jit(solution)/shard_map/all_to_all | solution.py:127
  23.7 149.1 %reduce-scatter.5.cloned.1.call-start = ((), (), s32[]{:S(2)}) async-start(), calls=%async_computation.5 | async-start | bytes 4718592 | tf_op jit(solution)/shard_map/reduce_scatter | solution.py:142
  99.6 8.9 %copy-start.5 = (f32[128]{0:T(128)S(1)}, f32[128]{0:T(128)}, u32[]{:S(2)}) copy-start(f32[128]{0:T(128)} %param.19) | copy-start | bytes 1540
  99.7 114.2 %reduce-scatter.3.cloned.1.call-start = ((), (), s32[]{:S(2)}) async-start(), calls=%async_computation.4 | async-start | bytes 3538944 | tf_op jit(solution)/shard_map/reduce_scatter | solution.py:82
  136.5 3.9 %copy-start.1 = (f32[768,1536]{1,0:T(8,128)S(1)}, f32[768,1536]{1,0:T(8,128)}, u32[]{:S(2)}) copy-start(f32[768,1536]{1,0:T(8,128)} %get-tuple-element.258) | copy-start | bytes 14155780 | tf_op jit(solution)/shard_map/while
  145.6 3.9 %copy-start.1 = (f32[768,1536]{1,0:T(8,128)S(1)}, f32[768,1536]{1,0:T(8,128)}, u32[]{:S(2)}) copy-start(f32[768,1536]{1,0:T(8,128)} %get-tuple-element.258) | copy-start | bytes 14155780 | tf_op jit(solution)/shard_map/while
  154.6 3.8 %copy-start.1 = (f32[768,1536]{1,0:T(8,128)S(1)}, f32[768,1536]{1,0:T(8,128)}, u32[]{:S(2)}) copy-start(f32[768,1536]{1,0:T(8,128)} %get-tuple-element.258) | copy-start | bytes 14155780 | tf_op jit(solution)/shard_map/while
  163.5 3.8 %copy-start.1 = (f32[768,1536]{1,0:T(8,128)S(1)}, f32[768,1536]{1,0:T(8,128)}, u32[]{:S(2)}) copy-start(f32[768,1536]{1,0:T(8,128)} %get-tuple-element.258) | copy-start | bytes 14155780 | tf_op jit(solution)/shard_map/while
  169.9 2.7 %copy-start.3 = (f32[384,2]{0,1:T(2,128)S(1)}, f32[384,2]{0,1:T(2,128)}, u32[]{:S(2)}) copy-start(f32[384,2]{0,1:T(2,128)} %param.24) | copy-start | bytes 9220
  174.7 10.0 %all-to-all-start.1 = ((bf16[4,4,8,2048]{3,2,0,1:T(8,128)(2,1)}), bf16[4,4,8,2048]{3,2,0,1:T(8,128)(2,1)S(1)}, u32[]{:S(2)}, u32[]{:S(2)}) async-start(bf16[4,4,8,2048]{3,2,0,1:T(8,128)(2,1)} %copy.52), calls=%async_computation.3 | async-start | bytes 1048576 | tf_op jit(solution)/shard_map/all_to_all | solution.py:145
Sparse Core Ops, SparseCore 0:
  99.8 50.3 reduce-scatter.4
  172.7 41.1 reduce-scatter.2
